TPU v7x, 32 devices: a whole 2x2x4 slice. The times are simulated.
32 devices in a mesh: sp: 8 (over z, y), tp: 4 (over x, core).
Axes of the slice: x: 2, y: 2, z: 4, core: 2. Of those that a mesh axis runs over, the one named last changes fastest.
Arguments:
- cotangent: bfloat16 [1024, 2048], P('sp', 'tp'), may hold values from -6 to 6
- mixer_out: bfloat16 [1024, 2048], P('sp', 'tp'), may hold values from -6 to 6
- route_ids: int32 [1024, 2], P('sp'), may hold values from 0 to 7, all different within a row; in each aligned block of 128 rows (0 to 127, 128 to 255, ...) at most 64 rows name the same one
- route_weights: float32 [1024, 2], P('sp'), may hold values from 0.2 to 1
- conv_out: bfloat16 [1024, 2048], P('sp', 'tp'), may hold values from -6 to 6
- recur_gate: bfloat16 [1024, 2048], P('sp', 'tp'), may hold values from 0.007 to 1
- input_gate: bfloat16 [1024, 2048], P('sp', 'tp'), may hold values from 0.099609375 to 0.8984375
- gate_pre: bfloat16 [1024, 2048], P('sp', 'tp'), may hold values from -6 to 6
- states_before: bfloat16 [1024, 2048], P('sp', 'tp'), may hold values from -4 to 4
- decay_rate: float32 [2048], P('tp'), may hold values from 4e-07 to 0.008
- out_proj: bfloat16 [2048, 2048], P(None, 'tp'), may hold values from -0.125 to 0.125
- recur_map: bfloat16 [4, 512, 512], P('tp'), may hold values from -0.25 to 0.25
- input_map: bfloat16 [4, 512, 512], P('tp'), may hold values from -0.25 to 0.25
- expert_gate: bfloat16 [8, 2048, 1024], P('sp', None, 'tp'), may hold values from -0.125 to 0.125
- expert_up: bfloat16 [8, 2048, 1024], P('sp', None, 'tp'), may hold values from -0.125 to 0.125
- expert_down: bfloat16 [8, 1024, 2048], P('sp', 'tp'), may hold values from -0.1875 to 0.1875
Outputs:
- grad_expert_gate: bfloat16 [8, 2048, 1024], P('sp', None, 'tp')
- grad_expert_up: bfloat16 [8, 2048, 1024], P('sp', None, 'tp')
- grad_expert_down: bfloat16 [8, 1024, 2048], P('sp', 'tp')
- grad_out_proj: float32 [2048, 2048], P('sp', 'tp')
- grad_conv: bfloat16 [1024, 2048], P('sp', 'tp')
- grad_gate_pre: bfloat16 [1024, 2048], P('sp', 'tp')
Inputs may be any that keep to these rules, and one draw needn't show every extreme that they name: `route_ids`: the two experts of a token differ. In every aligned block of 128 tokens no expert is named by more than 64 routes, and in some block some expert by exactly 64.
All inputs are finite; a program needn't handle non-finite values.
Results may differ from a plain program's by a relative error of at most 0.0093.
Values may be sent and summed in bfloat16 or wider, within the bound.
A program may use at most 64 MiB of HBM per device.

v0:
```python
import functools

import jax
import jax.numpy as jnp
from jax import lax
from jax.experimental import pallas as pl
from jax.experimental.pallas import tpu as pltpu
from jax.sharding import PartitionSpec as P

MESH = pl.DeviceIdType.MESH
VMEM = pl.BlockSpec(memory_space=pltpu.VMEM)
DMA = pltpu.SemaphoreType.DMA


def bits_of(count):
    found, bit = [], 1
    while bit < count:
        found.insert(0, bit)
        bit *= 2
    return found


def low_bit(mask):
    return mask & -mask


def flip(index, mask):
    bit = 1
    while bit <= mask:
        if mask & bit:
            index = index + bit - 2 * bit * lax.rem(lax.div(index, bit), 2)
        bit *= 2
    return index


def window(index, width):
    return pl.ds(pl.multiple_of(index * width, width), width)


def remote(source, target, send_sem, recv_sem, device):
    return pltpu.make_async_remote_copy(
        src_ref=source,
        dst_ref=target,
        send_sem=send_sem,
        recv_sem=recv_sem,
        device_id=device,
        device_id_type=MESH,
    )


def greet(peers):
    barrier = pltpu.get_barrier_semaphore()
    for peer in peers:
        pl.semaphore_signal(barrier, inc=1, device_id=peer, device_id_type=MESH)
    pl.semaphore_wait(barrier, len(peers))


def relays_of(count):
    masks = [mask for mask in range(1, count) if mask != low_bit(mask)]
    return sorted(masks, key=lambda mask: (bin(mask).count("1"), -mask))


def call(kernel, out_shape, scratch, ident, *operands):
    return pl.pallas_call(
        kernel,
        out_shape=out_shape,
        in_specs=[VMEM] * len(operands),
        out_specs=jax.tree.map(lambda _: VMEM, out_shape),
        scratch_shapes=scratch,
        compiler_params=pltpu.CompilerParams(
            collective_id=ident, has_side_effects=True, vmem_limit_bytes=48 * 1024 * 1024
        ),
    )(*operands)


def dispatch_kernel(n_sp, n_tp, rows, cots, got_rows, got_cots, own_sem, sa, ra, st, rt):
    s, t = lax.axis_index("sp"), lax.axis_index("tp")
    width = rows.shape[-1]
    kinds = ((rows, got_rows), (cots, got_cots))
    greet(
        [(flip(s, m), t) for m in range(1, n_sp)] + [(s, flip(t, b)) for b in bits_of(n_tp)]
    )

    def own(kind):
        source, target = kinds[kind]
        return pltpu.make_async_copy(
            source.at[s], target.at[s, :, window(t, width)], own_sem.at[kind]
        )

    def to_expert(kind, m):
        source, target = kinds[kind]
        q = flip(s, m)
        return remote(
            source.at[q], target.at[s, :, window(t, width)], sa.at[kind, m], ra.at[kind, m], (q, t)
        )

    def share(kind, m, k):
        bit = low_bit(k)
        block = kinds[kind][1].at[flip(s, m), :, window(flip(t, k - bit), width)]
        return remote(block, block, st.at[kind, m, k], rt.at[kind, m, k], (s, flip(t, bit)))

    seen = set()

    def forward(m):
        for kind in range(2):
            for k in relays_of(n_tp):
                before = k - low_bit(k)
                if (kind, m, before) not in seen:
                    share(kind, m, before).wait_recv()
                    seen.add((kind, m, before))
                share(kind, m, k).start()

    for kind in range(2):
        own(kind).start()
    for m in range(1, n_sp):
        for kind in range(2):
            to_expert(kind, m).start()
    for m in range(n_sp):
        for kind in range(2):
            if m == 0:
                own(kind).wait()
            else:
                to_expert(kind, m).wait_recv()
            for bit in bits_of(n_tp):
                share(kind, m, bit).start()
        if m > 0:
            forward(m - 1)
    forward(n_sp - 1)
    for kind in range(2):
        for m in range(n_sp):
            if m > 0:
                to_expert(kind, m).wait_send()
            for k in range(1, n_tp):
                share(kind, m, k).wait_send()
                if (kind, m, k) not in seen:
                    share(kind, m, k).wait_recv()


def combine_kernel(
    n_sp, n_tp, part, mixed, base, pick, out, mixed_all, half, xsend, xrecv, back, ret,
    own_sem, sh, rh, sx, rx, sb, rb, sg, rg, st, rt,
):
    s, t = lax.axis_index("sp"), lax.axis_index("tp")
    width = ret.shape[-1]
    pair, across = flip(t, 1), flip(t, 2)
    greet(
        [(flip(s, m), t) for m in range(1, n_sp)] + [(s, flip(t, b)) for b in bits_of(n_tp)]
    )

    def to_pair(slot):
        chunk = flip(pair, 2) if slot == 0 else pair
        return remote(
            part.at[:, :, window(chunk, width)], half.at[slot], sh.at[slot], rh.at[slot], (s, pair)
        )

    def cross(m):
        q = flip(s, m)
        return remote(xsend.at[q], xrecv.at[q], sx.at[m], rx.at[m], (s, across))

    def give(m):
        q = flip(s, m)
        return remote(back.at[q], ret.at[s], sb.at[m], rb.at[m], (q, t))

    def gather(k):
        bit = low_bit(k)
        block = flip(s, k - bit)
        source = mixed if k == bit else mixed_all.at[block]
        return remote(source, mixed_all.at[block], sg.at[k], rg.at[k], (flip(s, bit), t))

    seen = set()

    def forward(masks):
        for k in masks:
            before = k - low_bit(k)
            if before not in seen:
                gather(before).wait_recv()
                seen.add(before)
            gather(k).start()

    to_pair(0).start()
    to_pair(1).start()
    own = pltpu.make_async_copy(mixed, mixed_all.at[s], own_sem)
    own.start()
    for bit in bits_of(n_sp):
        gather(bit).start()
    order = list(range(n_sp - 1, -1, -1))
    to_pair(0).wait_recv()
    for m in order:
        q = flip(s, m)
        xsend[q] = (
            part[q, :, window(across, width)].astype(jnp.float32) + half[0, q].astype(jnp.float32)
        ).astype(jnp.bfloat16)
        cross(m).start()
    to_pair(1).wait_recv()
    relays = relays_of(n_sp)
    early = [k for k in relays if bin(k).count("1") == 2]
    forward(early)
    for place, m in enumerate(order):
        q = flip(s, m)
        cross(m).wait_recv()
        total = (
            part[q, :, window(t, width)].astype(jnp.float32)
            + half[1, q].astype(jnp.float32)
            + xrecv[q].astype(jnp.float32)
        ).astype(jnp.bfloat16)
        if m == 0:
            ret[s] = total
        else:
            back[q] = total
            give(m).start()
        if place == n_sp // 2:
            forward([k for k in relays if k not in early])
    total = base[...].astype(jnp.float32)
    for m in range(n_sp):
        q = flip(s, m)
        if m > 0:
            give(m).wait_recv()
        total = total + contract_rows(pick[q], ret[q])
    out[:, window(t, width)] = total.astype(jnp.bfloat16)

    def share(k):
        bit = low_bit(k)
        block = out.at[:, window(flip(t, k - bit), width)]
        return remote(block, block, st.at[k], rt.at[k], (s, flip(t, bit)))

    for bit in bits_of(n_tp):
        share(bit).start()
    shared = set()
    for k in relays_of(n_tp):
        before = k - low_bit(k)
        if before not in shared:
            share(before).wait_recv()
            shared.add(before)
        share(k).start()
    for k in range(1, n_tp):
        share(k).wait_send()
        if k not in shared:
            share(k).wait_recv()
    own.wait()
    for slot in range(2):
        to_pair(slot).wait_send()
    for m in range(n_sp):
        cross(m).wait_send()
        if m > 0:
            give(m).wait_send()
            gather(m).wait_send()
            if m not in seen:
                gather(m).wait_recv()


def scan_kernel(
    n_sp, flipped, drive, decay, state_grad, pieces, weight, carry, carries,
    own_sem, sa, ra, sc, rc,
):
    s, t = lax.axis_index("sp"), lax.axis_index("tp")
    rows = drive.shape[0]
    share = flipped.shape[0] // n_sp
    greet([(flip(s, m), t) for m in range(1, n_sp)])

    def piece(m):
        q = flip(s, m)
        return remote(
            flipped.at[window(q, share)], pieces.at[:, window(s, rows)], sa.at[m], ra.at[m], (q, t)
        )

    def send_carry(m):
        return remote(carry, carries.at[s], sc.at[m], rc.at[m], (flip(s, m), t))

    own = pltpu.make_async_copy(
        flipped.at[window(s, share)], pieces.at[:, window(s, rows)], own_sem
    )
    own.start()

    def lap(step, held):
        grad, product = held
        row = rows - 1 - step
        grad = drive[pl.ds(row, 1), :] + grad
        product_here = product
        state_grad[pl.ds(row, 1), :] = grad
        weight[pl.ds(row, 1), :] = product_here
        now = decay[pl.ds(row, 1), :]
        return (now * grad, now * product_here)

    zero = jnp.zeros((1, drive.shape[1]), jnp.float32)
    start, span = lax.fori_loop(0, rows, lap, (zero, zero + 1.0), unroll=8)
    carry[0:1, :] = span
    carry[1:2, :] = start
    for m in range(1, n_sp):
        send_carry(m).start()
    for m in range(1, n_sp):
        piece(m).start()
    for m in range(1, n_sp):
        send_carry(m).wait_recv()
    incoming = zero
    for later in range(n_sp - 1, 0, -1):
        longer = carries[later, 1:2, :] + carries[later, 0:1, :] * incoming
        incoming = jnp.where(later > s, longer, incoming)
    state_grad[...] = state_grad[...] + weight[...] * incoming
    own.wait()
    for m in range(1, n_sp):
        send_carry(m).wait_send()
        piece(m).wait_send()
        piece(m).wait_recv()


def silu_parts(values):
    sig = jax.nn.sigmoid(values)
    return (values * sig, sig * (1.0 + values * (1.0 - sig)))


def route_slots(route_block, experts, capacity):
    flat_ids = route_block.reshape(-1)
    onehot = (flat_ids[:, None] == jnp.arange(experts, dtype=jnp.int32)[None, :]).astype(jnp.int32)
    before = jnp.cumsum(onehot, axis=0) - onehot
    slot_rank = jnp.sum(before * onehot, axis=1)
    return flat_ids * capacity + slot_rank


def contract_rows(left, right):
    return lax.dot_general(
        left, right, (((0,), (0,)), ((), ())), preferred_element_type=jnp.float32
    )


def body(
    cotangent,
    mixer_out,
    route_ids,
    route_weights,
    conv_out,
    recur_gate,
    input_gate,
    gate_pre,
    states_before,
    decay_rate,
    out_proj,
    recur_map,
    input_map,
    expert_gate,
    expert_up,
    expert_down,
):
    row_count = cotangent.shape[0]
    experts = lax.axis_size("sp")
    capacity = 4 * row_count // experts
    slot_pos = route_slots(route_ids, experts, capacity).reshape(row_count, 2)
    slot_range = jnp.arange(experts * capacity, dtype=jnp.int32)[:, None]
    hit_first = slot_range == slot_pos[None, :, 0]
    hit_second = slot_range == slot_pos[None, :, 1]
    dispatch = (hit_first | hit_second).astype(jnp.bfloat16)
    slot_weight = jnp.sum(
        jnp.where(hit_first, route_weights[None, :, 0], 0.0)
        + jnp.where(hit_second, route_weights[None, :, 1], 0.0),
        axis=1,
    )
    send_rows = jnp.dot(dispatch, mixer_out, preferred_element_type=jnp.float32).astype(
        jnp.bfloat16
    )
    send_cot = (
        jnp.dot(dispatch, cotangent, preferred_element_type=jnp.float32) * slot_weight[:, None]
    ).astype(jnp.bfloat16)
    tps = lax.axis_size("tp")
    features = tps * cotangent.shape[1]
    slots = experts * capacity
    blocks = (experts, capacity, features)
    got_rows, got_cot = call(
        functools.partial(dispatch_kernel, experts, tps),
        [jax.ShapeDtypeStruct(blocks, jnp.bfloat16)] * 2,
        [
            DMA((2,)),
            DMA((2, experts)),
            DMA((2, experts)),
            DMA((2, experts, tps)),
            DMA((2, experts, tps)),
        ],
        0,
        send_rows.reshape(experts, capacity, -1),
        send_cot.reshape(experts, capacity, -1),
    )
    got_rows, got_cot = (got_rows.reshape(slots, features), got_cot.reshape(slots, features))
    w_gate = expert_gate[0]
    w_up = expert_up[0]
    w_down = expert_down[0]
    pre_gate = jnp.dot(got_rows, w_gate, preferred_element_type=jnp.float32)
    pre_up = jnp.dot(got_rows, w_up, preferred_element_type=jnp.float32)
    gate_act, slope = silu_parts(pre_gate)
    active = (gate_act * pre_up).astype(jnp.bfloat16)
    d_active = lax.dot_general(
        got_cot, w_down, (((1,), (1,)), ((), ())), preferred_element_type=jnp.float32
    )
    grad_down = contract_rows(active, got_cot).astype(jnp.bfloat16)
    d_gate = (d_active * pre_up * slope).astype(jnp.bfloat16)
    d_up = (d_active * gate_act).astype(jnp.bfloat16)
    grad_gate = contract_rows(got_rows, d_gate).astype(jnp.bfloat16)
    grad_up = contract_rows(got_rows, d_up).astype(jnp.bfloat16)
    partial_grad = lax.dot_general(
        d_gate, w_gate, (((1,), (1,)), ((), ())), preferred_element_type=jnp.float32
    ) + lax.dot_general(d_up, w_up, (((1,), (1,)), ((), ())), preferred_element_type=jnp.float32)
    channels = conv_out.shape[1]
    rate = decay_rate[None, :]
    recur_f = recur_gate.astype(jnp.float32)
    input_f = input_gate.astype(jnp.float32)
    conv_f = conv_out.astype(jnp.float32)
    before_f = states_before.astype(jnp.float32)
    log_decay = -8.0 * recur_f * rate
    decay_now = jnp.exp(log_decay)
    position = lax.axis_index("sp") * row_count + jnp.arange(row_count, dtype=jnp.int32)
    at_start = (position == 0)[:, None]
    norm_factor = jnp.where(at_start, 1.0, jnp.sqrt(-jnp.expm1(2.0 * log_decay)))
    norm_slope = jnp.where(at_start, 0.0, -jnp.exp(2.0 * log_decay) / norm_factor)
    drive = input_f * conv_f
    state = decay_now * before_f + norm_factor * drive
    gate, gelu_back = jax.vjp(jax.nn.gelu, gate_pre.astype(jnp.float32))
    mixed = (state * gate).astype(jnp.bfloat16)
    block = (experts, capacity, cotangent.shape[1])
    pair_sems, own_sems = (DMA((2,)), DMA((experts,)))
    tp_sems = DMA((tps,))
    out_grad, mixed_all = call(
        functools.partial(combine_kernel, experts, tps),
        [
            jax.ShapeDtypeStruct((row_count, features), jnp.bfloat16),
            jax.ShapeDtypeStruct((experts, row_count, channels), jnp.bfloat16),
        ],
        [
            pltpu.VMEM((2, *block), jnp.bfloat16),
            pltpu.VMEM(block, jnp.bfloat16),
            pltpu.VMEM(block, jnp.bfloat16),
            pltpu.VMEM(block, jnp.bfloat16),
            pltpu.VMEM(block, jnp.bfloat16),
            DMA,
            pair_sems,
            pair_sems,
            *([own_sems] * 6),
            tp_sems,
            tp_sems,
        ],
        1,
        partial_grad.astype(jnp.bfloat16).reshape(blocks),
        mixed,
        cotangent,
        dispatch.reshape(experts, capacity, row_count),
    )
    d_mixed = jnp.dot(out_grad, out_proj, preferred_element_type=jnp.float32)
    state_grad, pieces = call(
        functools.partial(scan_kernel, experts),
        [
            jax.ShapeDtypeStruct((row_count, channels), jnp.float32),
            jax.ShapeDtypeStruct((features // experts, experts * row_count), jnp.bfloat16),
        ],
        [
            pltpu.VMEM((row_count, channels), jnp.float32),
            pltpu.VMEM((2, channels), jnp.float32),
            pltpu.VMEM((experts, 2, channels), jnp.float32),
            DMA,
            *([own_sems] * 4),
        ],
        2,
        out_grad.T,
        d_mixed * gate,
        decay_now,
    )
    grad_out_proj = jnp.dot(
        pieces,
        mixed_all.reshape(experts * row_count, channels),
        preferred_element_type=jnp.float32,
    )
    grad_gate_pre = gelu_back(d_mixed * state)[0].astype(jnp.bfloat16)
    d_log = state_grad * (decay_now * before_f + norm_slope * drive)
    d_recur_pre = (d_log * (-8.0 * rate) * recur_f * (1.0 - recur_f)).astype(jnp.bfloat16)
    d_input_pre = (state_grad * norm_factor * conv_f * input_f * (1.0 - input_f)).astype(
        jnp.bfloat16
    )
    groups = recur_map.shape[0]
    width = recur_map.shape[1]
    through_recur = jnp.einsum(
        "tbj,bij->tbi",
        d_recur_pre.reshape(row_count, groups, width),
        recur_map,
        preferred_element_type=jnp.float32,
    )
    through_input = jnp.einsum(
        "tbj,bij->tbi",
        d_input_pre.reshape(row_count, groups, width),
        input_map,
        preferred_element_type=jnp.float32,
    )
    grad_conv = (
        state_grad * norm_factor * input_f
        + (through_recur + through_input).reshape(row_count, channels)
    ).astype(jnp.bfloat16)
    return (
        grad_gate[None],
        grad_up[None],
        grad_down[None],
        grad_out_proj,
        grad_conv,
        grad_gate_pre,
    )


def solution(mesh):
    placed = (
        P("sp", "tp"),
        P("sp", "tp"),
        P("sp", None),
        P("sp", None),
        P("sp", "tp"),
        P("sp", "tp"),
        P("sp", "tp"),
        P("sp", "tp"),
        P("sp", "tp"),
        P("tp"),
        P(None, "tp"),
        P("tp", None, None),
        P("tp", None, None),
        P("sp", None, "tp"),
        P("sp", None, "tp"),
        P("sp", "tp", None),
    )
    return jax.shard_map(
        body,
        mesh=mesh,
        in_specs=placed,
        out_specs=(
            P("sp", None, "tp"),
            P("sp", None, "tp"),
            P("sp", "tp", None),
            P("sp", "tp"),
            P("sp", "tp"),
            P("sp", "tp"),
        ),
        check_vma=False,
    )
```

profile of v0, /device:TPU:0, one launch (start us, length us, event | category | flops | bytes accessed | tf_op | source)
XLA Modules:
  0.0 110.6 jit_solution(7573020887260942608)
XLA Ops:
  0.6 0.0 copy-start
  0.6 0.0 copy-start.5
  0.7 0.9 copy.38
  1.6 0.1 eq.94
  1.8 0.6 reduce-window.6
  2.3 0.2 slice_reduce_fusion
  2.6 0.1 eq.90
  2.7 0.1 fusion.68
  2.8 0.1 reduce_sum.21
  3.0 0.1 copy.40
  3.0 0.7 multiply_add_fusion.2
  3.8 1.2 %convolution_convert_fusion.3 = bf16[512,512]{1,0:T(8,128)(2,1)S(1)} fusion(bf16[128,512]{1,0:T(8,128)(2,1)} %param.17, s32[128]{0:T(128)S(1)} %get-tuple-element.26, s32[128]{0:T(128)S(1)} %get-tuple-element.25), kind=kOutput, calls=%fused_computation.9 | convolution fusion | flops 67567616 | bytes 656384 | tf_op jit(solution)/shard_map/dot_general | solution.py:356
  5.0 0.8 slice_bitcast_fusion.1
  5.7 0.1 add_reduce_fusion
  5.9 1.2 %fusion.3 = bf16[512,512]{1,0:T(8,128)(2,1)S(1)} fusion(bf16[128,512]{1,0:T(8,128)(2,1)} %base.1, f32[512]{0:T(512)S(1)} %add_reduce_fusion, s32[128]{0:T(128)S(1)} %get-tuple-element.26, s32[128]{0:T(128)S(1)} %get-tuple-element.25), kind=kOutput, calls=%fused_computation.8 | convolution fusion | flops 67829760 | bytes 658432 | tf_op jit(solution)/shard_map/dot_general | solution.py:360
  7.1 35.4 %shard_map.199 = (bf16[8,64,2048]{2,1,0:T(8,128)(2,1)S(1)}, bf16[8,64,2048]{2,1,0:T(8,128)(2,1)S(1)}) custom-call(bf16[8,64,512]{2,1,0:T(8,128)(2,1)S(1)} %bitcast.67, bf16[8,64,512]{2,1,0:T(8,128)(2,1)S(1)} %bitcast.68), custom_call_target="tpu_custom_call" | custom-call | tf_op jit(solution)/shard_map/pallas_call | solution.py:64
  42.5 0.0 copy-start.6
  42.5 0.0 copy-done.5
  42.5 0.7 fusion.8
  43.2 0.5 copy-done.6
  43.7 0.0 copy-start.15
  43.7 0.7 fusion.11
  44.4 0.5 copy-done.15
  45.0 0.8 multiply_convert_fusion.1
  45.8 1.7 %fusion = bf16[1,2048,256]{2,1,0:T(8,128)(2,1)} fusion(bf16[512,2048]{1,0:T(8,128)(2,1)S(1)} %bitcast.75, bf16[512,256]{1,0:T(8,128)(2,1)S(1)} %get-tuple-element.19), kind=kOutput, calls=%fused_computation.4 | convolution fusion | flops 537395200 | bytes 3407872 | tf_op jit(solution)/shard_map/dot_general | solution.py:320
  47.5 1.7 %fusion.1 = bf16[1,2048,256]{2,1,0:T(8,128)(2,1)} fusion(bf16[512,2048]{1,0:T(8,128)(2,1)S(1)} %bitcast.76, bf16[512,256]{1,0:T(8,128)(2,1)S(1)} %get-tuple-element.18), kind=kOutput, calls=%fused_computation.5 | convolution fusion | flops 537395200 | bytes 3407872 | tf_op jit(solution)/shard_map/dot_general | solution.py:320
  49.2 1.7 %fusion.2 = bf16[1,256,2048]{2,1,0:T(8,128)(2,1)} fusion(bf16[512,2048]{1,0:T(8,128)(2,1)S(1)} %bitcast.70, f32[512,256]{1,0:T(8,128)S(1)} %fusion.11, f32[512,256]{1,0:T(8,128)S(1)} %fusion.8), kind=kOutput, calls=%fused_computation.6 | convolution fusion | flops 538181632 | bytes 4194304 | tf_op jit(solution)/shard_map/dot_general | solution.py:320
  51.0 0.7 fusion.6
  51.7 0.0 copy-start.14
  51.7 0.0 copy-start.7
  51.7 0.0 copy-start.8
  51.7 0.0 copy-start.9
  51.8 0.0 copy-start.10
  51.8 0.0 copy-start.12
  51.8 0.0 copy-start.4
  51.8 2.1 %add_convert_fusion = bf16[512,2048]{1,0:T(8,128)(2,1)} fusion(f32[512,2048]{1,0:T(8,128)S(1)} %fusion.6, bf16[512,256]{1,0:T(8,128)(2,1)S(1)} %get-tuple-element.18, bf16[1,2048,256]{2,1,0:T(8,128)(2,1)S(1)} %copy-done.6), kind=kOutput, calls=%fused_computation | convolution fusion | flops 538968064 | bytes 7602176 | tf_op jit(solution)/shard_map/dot_general | solution.py:398
  53.9 0.0 copy-done.14
  53.9 0.0 copy-done.7
  53.9 0.0 copy-done.8
  53.9 0.0 copy-done.9
  53.9 0.0 copy-done.10
  53.9 0.0 copy-done.12
  54.0 0.4 multiply_convert_fusion.4.mixed
  54.3 0.1 or_convert_fusion.pick
  54.5 0.0 copy-done.4
  54.5 0.0 copy-start.1
  54.5 1.6 %copy-done.1 = bf16[512,2048]{1,0:T(8,128)(2,1)S(1)} copy-done((bf16[512,2048]{1,0:T(8,128)(2,1)S(1)}, bf16[512,2048]{1,0:T(8,128)(2,1)}, u32[]{:S(2)}) %copy-start.1) | copy-done | bytes 2097176
  56.1 32.2 %shard_map.200 = (bf16[128,2048]{1,0:T(8,128)(2,1)S(1)}, bf16[8,128,512]{2,1,0:T(8,128)(2,1)S(1)}) custom-call(bf16[8,64,2048]{2,1,0:T(8,128)(2,1)S(1)} %bitcast.66, bf16[128,512]{1,0:T(8,128)(2,1)S(1)} %multiply_convert_fusion.4.mixed, bf16[128,512]{1,0:T(8,128)(2,1)S(1)} %copy-done.4, bf16[8,64,128]{2,1,0:T(8,128)(2,1)S(1)} %or_convert_fusion.pick), custom_call_target="tpu_custom_call" | custom-call | tf_op jit(solution)/shard_map/pallas_call | solution.py:64
  88.3 0.0 copy-start.2
  88.3 1.0 copy-done.2
  89.3 0.3 copy.41
  89.6 0.0 copy-done
  89.6 0.0 copy-start.3
  89.6 2.5 %fusion.35 = (bf16[128,512]{1,0:T(8,128)(2,1)}, f32[128,512]{1,0:T(8,128)S(1)}, f32[128,512]{1,0:T(8,128)S(1)}) fusion(bf16[128,512]{1,0:T(8,128)(2,1)S(1)} %copy-done.7, bf16[128,512]{1,0:T(8,128)(2,1)S(1)} %copy-done.9, bf16[128,512]{1,0:T(8,128)(2,1)} %param.22, pred[128]{0:T(512)(128)(4,1)S(1)} %add_compare_fusion, bf16[128,512]{1,0:T(8,128)(2,1)S(1)} %copy-done.8, ...), kind=kOutput, calls=%fused_computation.59 | convolution fusion | flops 270794752 | bytes 3934336 | tf_op jit(solution)/shard_map/dot_general | solution.py:443
  92.1 15.5 %shard_map.201 = (f32[128,512]{1,0:T(8,128)S(1)}, bf16[256,1024]{1,0:T(8,128)(2,1)S(1)}) custom-call(bf16[2048,128]{1,0:T(8,128)(2,1)S(1)} %bitcast.71, f32[128,512]{1,0:T(8,128)S(1)} %get-tuple-element.21.drive, f32[128,512]{1,0:T(8,128)S(1)} %get-tuple-element.22.decay), custom_call_target="tpu_custom_call" | custom-call | tf_op jit(solution)/shard_map/pallas_call | solution.py:64
  107.6 0.0 copy-done.3
  107.6 0.0 copy-start.17
  107.6 1.2 %fusion.76 = f32[256,512]{1,0:T(8,128)} fusion(bf16[256,1024]{1,0:T(8,128)(2,1)S(1)} %get-tuple-element.15, bf16[1024,512]{1,0:T(8,128)(2,1)S(1)} %bitcast.72), kind=kOutput, calls=%fused_computation.113 | convolution fusion | flops 268435456 | bytes 2097152 | tf_op jit(solution)/shard_map/dot_general | solution.py:462
  108.8 0.0 copy-done.11
  108.9 0.0 copy-done.13
  108.9 0.0 copy-done.16
  108.9 0.5 fusion.16
  109.4 0.0 copy-done.17
  109.4 1.2 %fusion.5 = bf16[128,512]{1,0:T(8,128)(2,1)} fusion(f32[128,512]{1,0:T(8,128)S(1)} %fusion.16, bf16[1,512,512]{2,1,0:T(8,128)(2,1)S(1)} %copy-done.17, bf16[128,512]{1,0:T(8,128)(2,1)S(1)} %copy-done.11, bf16[128,512]{1,0:T(8,128)(2,1)S(1)} %copy-done.9, f32[128,512]{1,0:T(8,128)S(1)} %get-tuple-element.17, bf16[128,512]{1,0:T(8,128)(2,1)S(1)} %copy-done.13, ...), kind=kOutput, calls=%fused_computation.12 | convolution fusion | flops 68681728 | bytes 1575040 | tf_op jit(solution)/shard_map/tbj,bij->tbi/dot_general | solution.py:481
  (10 shorter events, 0.1 us)
Async XLA Ops:
  0.6 88.9 %copy-start = (bf16[2048,512]{1,0:T(8,128)(2,1)S(1)}, bf16[2048,512]{1,0:T(8,128)(2,1)}, u32[]{:S(2)}) copy-start(bf16[2048,512]{1,0:T(8,128)(2,1)} %param.26) | copy-start | bytes 6291460
  0.6 41.9 %copy-start.5 = (bf16[1,2048,256]{2,1,0:T(8,128)(2,1)S(1)}, bf16[1,2048,256]{2,1,0:T(8,128)(2,1)}, u32[]{:S(2)}) copy-start(bf16[1,2048,256]{2,1,0:T(8,128)(2,1)} %param.29) | copy-start | bytes 3145732
  42.5 1.2 %copy-start.6 = (bf16[1,2048,256]{2,1,0:T(8,128)(2,1)S(1)}, bf16[1,2048,256]{2,1,0:T(8,128)(2,1)}, u32[]{:S(2)}) copy-start(bf16[1,2048,256]{2,1,0:T(8,128)(2,1)} %param.30) | copy-start | bytes 3145732
  43.7 1.2 %copy-start.15 = (bf16[1,256,2048]{2,1,0:T(8,128)(2,1)S(1)}, bf16[1,256,2048]{2,1,0:T(8,128)(2,1)}, u32[]{:S(2)}) copy-start(bf16[1,256,2048]{2,1,0:T(8,128)(2,1)} %param.31) | copy-start | bytes 3145732
  51.7 2.2 %copy-start.14 = (f32[512]{0:T(512)S(1)}, f32[512]{0:T(512)}, u32[]{:S(2)}) copy-start(f32[512]{0:T(512)} %param.25) | copy-start | bytes 6148
  51.7 2.2 %copy-start.7 = (bf16[128,512]{1,0:T(8,128)(2,1)S(1)}, bf16[128,512]{1,0:T(8,128)(2,1)}, u32[]{:S(2)}) copy-start(bf16[128,512]{1,0:T(8,128)(2,1)} %param.23) | copy-start | bytes 393220
  51.7 2.2 %copy-start.8 = (bf16[128,512]{1,0:T(8,128)(2,1)S(1)}, bf16[128,512]{1,0:T(8,128)(2,1)}, u32[]{:S(2)}) copy-start(bf16[128,512]{1,0:T(8,128)(2,1)} %param.24) | copy-start | bytes 393220
  51.7 2.2 %copy-start.9 = (bf16[128,512]{1,0:T(8,128)(2,1)S(1)}, bf16[128,512]{1,0:T(8,128)(2,1)}, u32[]{:S(2)}) copy-start(bf16[128,512]{1,0:T(8,128)(2,1)} %param.20) | copy-start | bytes 393220
  51.8 2.2 %copy-start.10 = (bf16[128,512]{1,0:T(8,128)(2,1)S(1)}, bf16[128,512]{1,0:T(8,128)(2,1)}, u32[]{:S(2)}) copy-start(bf16[128,512]{1,0:T(8,128)(2,1)} %param.22) | copy-start | bytes 393220
  51.8 2.2 %copy-start.12 = (bf16[128,512]{1,0:T(8,128)(2,1)S(1)}, bf16[128,512]{1,0:T(8,128)(2,1)}, u32[]{:S(2)}) copy-start(bf16[128,512]{1,0:T(8,128)(2,1)} %param.21) | copy-start | bytes 393220
  51.8 2.7 %copy-start.4 = (bf16[128,512]{1,0:T(8,128)(2,1)S(1)}, bf16[128,512]{1,0:T(8,128)(2,1)}, u32[]{:S(2)}) copy-start(bf16[128,512]{1,0:T(8,128)(2,1)} %base.1) | copy-start | bytes 393220
  54.5 1.6 %copy-start.1 = (bf16[512,2048]{1,0:T(8,128)(2,1)S(1)}, bf16[512,2048]{1,0:T(8,128)(2,1)}, u32[]{:S(2)}) copy-start(bf16[512,2048]{1,0:T(8,128)(2,1)} %add_convert_fusion) | copy-start | bytes 6291460
  88.3 1.0 copy-start.2
  89.6 18.0 %copy-start.3 = (bf16[8,128,512]{2,1,0:T(8,128)(2,1)S(1)}, bf16[8,128,512]{2,1,0:T(8,128)(2,1)}, u32[]{:S(2)}) copy-start(bf16[8,128,512]{2,1,0:T(8,128)(2,1)} %copy-done.2) | copy-start | bytes 3145732
  92.1 16.8 %copy-start.11 = (bf16[128,512]{1,0:T(8,128)(2,1)S(1)}, bf16[128,512]{1,0:T(8,128)(2,1)}, u32[]{:S(2)}) copy-start(bf16[128,512]{1,0:T(8,128)(2,1)} %param.22) | copy-start | bytes 393220
  92.1 16.8 %copy-start.13 = (bf16[128,512]{1,0:T(8,128)(2,1)S(1)}, bf16[128,512]{1,0:T(8,128)(2,1)}, u32[]{:S(2)}) copy-start(bf16[128,512]{1,0:T(8,128)(2,1)} %param.21) | copy-start | bytes 393220
  92.1 16.8 %copy-start.16 = (bf16[1,512,512]{2,1,0:T(8,128)(2,1)S(1)}, bf16[1,512,512]{2,1,0:T(8,128)(2,1)}, u32[]{:S(2)}) copy-start(bf16[1,512,512]{2,1,0:T(8,128)(2,1)} %param.27) | copy-start | bytes 1572868
  107.6 1.8 %copy-start.17 = (bf16[1,512,512]{2,1,0:T(8,128)(2,1)S(1)}, bf16[1,512,512]{2,1,0:T(8,128)(2,1)}, u32[]{:S(2)}) copy-start(bf16[1,512,512]{2,1,0:T(8,128)(2,1)} %param.28) | copy-start | bytes 1572868
where the time goes:
time: 111 us
  Pallas kernels  83.1 us (75%)
  matrix products  18.1 us (16%)
  local copies, waits for them, and re-layouts  6.31 us (6%)
  other arithmetic  2.09 us (2%)
    pallas_call x3, Pallas kernels, call(): pl.pallas_call(kernel, out_shape=out_shape, in_specs=[VMEM] * len(operand...  83.1 us
    dot_general x3, matrix products, contract_rows(): lax.dot_general(left, right, (((0,), (0,)), ((), ())), preferred_element_...  5.21 us
    unnamed x37, local copies, waits for them, and re-layouts  4.58 us
    dot_general x1, matrix products, body(): d_mixed = jnp.dot(out_grad, out_proj, preferred_element_type=jnp.float32)  2.49 us

commit v1 on v0

--- a/solution.py
+++ b/solution.py
@@ -71,6 +71,671 @@
             collective_id=ident, has_side_effects=True, vmem_limit_bytes=48 * 1024 * 1024
         ),
     )(*operands)
+
+
+def along(index, table):
+    found = 0
+    for place, value in enumerate(table):
+        found = found + jnp.where(index == place, value, 0)
+    return found
+
+
+def abs_of(value):
+    return jnp.where(value < 0, -value, value)
+
+
+def nearest(count):
+    return [sorted(range(count), key=lambda other: (abs(other - z), other)) for z in range(count)]
+
+
+def contract_columns(left, right):
+    return lax.dot_general(
+        left, right, (((1,), (1,)), ((), ())), preferred_element_type=jnp.float32
+    )
+
+
+def expm1_of(values):
+    near = 1.0 / 362880.0
+    for factor in (40320.0, 5040.0, 720.0, 120.0, 24.0, 6.0, 2.0, 1.0):
+        near = near * values + 1.0 / factor
+    return jnp.where(jnp.abs(values) < 0.3, values * near, jnp.exp(values) - 1.0)
+
+
+def expert_kernel(
+    n_sp, n_tp, capacity,
+    rows_hbm, cots_hbm, ids_hbm, weights_hbm, conv_hbm, recur_hbm, input_hbm, gate_hbm,
+    before_hbm, rate_hbm, proj_hbm, w_gate_hbm, w_up_hbm, w_down_hbm,
+    mixed_all, pieces, grad_gate, grad_up, grad_down, state_grad, recur_part, input_part,
+    conv_part, grad_gate_pre,
+    rows, cots, ids, weights, conv, recur, inputs, gate_pre, before, rate, proj,
+    w_gate, w_up, w_down,
+    tok, meta, got, ybuf, act, dgate, dup, give_pair, mine, half,
+    xsend, xrecv, back, ret, pick, out, mixed, decay, gate, gate_part, drive, product, carry,
+    carries,
+    lsem, tss, trs, mss, mrs, yss, yrs, hss, hrs, pss, prs, css, crs, gss, grs,
+    zss, zrs, oss, ors, iss, irs, kss, krs, own_sem,
+):
+    s, t = lax.axis_index("sp"), lax.axis_index("tp")
+    n_y = 2
+    n_z = n_sp // n_y
+    z, y = lax.div(s, n_y), lax.rem(s, n_y)
+    beside = flip(s, 1)
+    pair, across = flip(t, 1), flip(t, 2)
+    tokens, width = rows.shape
+    chunk = n_y * capacity
+    f32, bf16 = jnp.float32, jnp.bfloat16
+    order = [along(z, [found[k] for found in nearest(n_z)]) for k in range(n_z)]
+
+    fetch = [
+        pltpu.make_async_copy(source, target, lsem.at[i])
+        for i, (source, target) in enumerate(
+            (
+                (rows_hbm, rows), (cots_hbm, cots), (ids_hbm, ids), (weights_hbm, weights),
+                (conv_hbm, conv), (recur_hbm, recur), (input_hbm, inputs), (gate_hbm, gate_pre),
+                (before_hbm, before), (rate_hbm, rate),
+                (w_gate_hbm, w_gate), (w_up_hbm, w_up), (w_down_hbm, w_down), (proj_hbm, proj),
+            )
+        )
+    ]
+    for copy in fetch:
+        copy.start()
+    barrier_peers = [(flip(s, m), t) for m in range(1, n_sp)]
+    barrier_peers += [(flip(s, m), flip(t, 2)) for m in range(1, n_sp)]
+    greet(barrier_peers + [(s, flip(t, b)) for b in bits_of(n_tp)])
+    for copy in fetch[:4]:
+        copy.wait()
+    ends = []
+
+    def begin(copy, valid=None):
+        ends.append((copy, valid))
+        if valid is None:
+            copy.start()
+        else:
+            pl.when(valid)(copy.start)
+
+    def spread(make, zb, first):
+        above, below = z + 1 < n_z, z >= 1
+        if not first:
+            above, below = (zb < z) & above, (zb > z) & below
+        begin(make(zb, z + 1, 0), above)
+        begin(make(zb, z - 1, 1), below)
+
+    def along_line(source, target, send_sem, recv_sem, z_to):
+        return remote(source, target, send_sem, recv_sem, (z_to * n_y + y, t))
+
+    def move_tokens(kind, zb, z_to, way, own):
+        target = tok.at[kind, zb]
+        source = (rows, cots)[kind] if own else target
+        return along_line(source, target, tss.at[kind, zb, way], trs.at[kind, zb], z_to)
+
+    def move_meta(zb, z_to, way):
+        return along_line(meta.at[zb], meta.at[zb], mss.at[zb, way], mrs.at[zb], z_to)
+
+    def move_mixed(zb, z_to, way, own):
+        target = mixed_all.at[zb * n_y + y]
+        source = mixed if own else target
+        return along_line(source, target, zss.at[zb, way], zrs.at[zb * n_y + y], z_to)
+
+    def mixed_beside(zb, own):
+        target = mixed_all.at[zb * n_y + y]
+        source = mixed if own else target
+        return remote(source, target, zss.at[zb, 2], zrs.at[zb * n_y + y], (beside, t))
+
+    def mixed_from_beside(zb):
+        target = mixed_all.at[zb * n_y + 1 - y]
+        return remote(mixed, target, zss.at[zb, 2], zrs.at[zb * n_y + 1 - y], (beside, t))
+
+    def slots(kind, block, quarter):
+        return got.at[kind, window(block, capacity), window(quarter, width)]
+
+    def to_beside(kind, zb):
+        return remote(
+            ybuf.at[kind, zb], slots(kind, zb * n_y + y, t),
+            yss.at[kind, zb], yrs.at[kind, zb], (beside, t),
+        )
+
+    def from_beside(kind, zb):
+        return remote(
+            ybuf.at[kind, zb], slots(kind, zb * n_y + 1 - y, t),
+            yss.at[kind, zb], yrs.at[kind, zb], (beside, t),
+        )
+
+    def share(kind, block, k):
+        bit = low_bit(k)
+        ref = slots(kind, block, flip(t, k - bit))
+        return remote(ref, ref, hss.at[kind, block, k], hrs.at[kind, block, k], (s, flip(t, bit)))
+
+    def arrived(kind, block, k):
+        ref = slots(kind, block, flip(t, k))
+        return remote(
+            ref, ref, hss.at[kind, block, k], hrs.at[kind, block, k], (s, flip(t, low_bit(k)))
+        )
+
+    table_rows = lax.broadcasted_iota(jnp.int32, (2 * n_sp, tokens), 0)
+    first_id, second_id = ids[0:1, :], ids[1:2, :]
+    hits = ((first_id == table_rows) | (second_id == table_rows)).astype(f32)
+    earlier = lax.broadcasted_iota(jnp.int32, (tokens, tokens), 0) < lax.broadcasted_iota(
+        jnp.int32, (tokens, tokens), 1
+    )
+    rank = jnp.dot(
+        hits.astype(bf16), earlier.astype(f32).astype(bf16), preferred_element_type=f32
+    )
+    rank = jnp.where(hits > 0.0, rank, -1.0)
+    weight_rows = table_rows - n_sp
+    weight = jnp.where(first_id == weight_rows, weights[0:1, :], 0.0) + jnp.where(
+        second_id == weight_rows, weights[1:2, :], 0.0
+    )
+    meta[z] = jnp.where(table_rows < n_sp, rank, weight)
+
+    spread(lambda zb, to, way: move_tokens(0, zb, to, way, True), z, True)
+    spread(move_meta, z, True)
+    spread(lambda zb, to, way: move_tokens(1, zb, to, way, True), z, True)
+
+    slot_index = lax.broadcasted_iota(jnp.int32, (capacity, tokens), 0).astype(f32)
+
+    def chosen(zb, expert):
+        return meta[zb, pl.ds(expert, 1), :] == slot_index
+
+    def compact(kind, k, valid=None):
+        zb = order[k]
+        block = zb * n_y + y
+        sends = (to_beside(kind, zb), share(kind, block, 2), share(kind, block, 1))
+        ends.extend((copy, valid) for copy in sends)
+
+        def work():
+            picks = jnp.concatenate(
+                [chosen(zb, s).astype(f32), chosen(zb, beside).astype(f32)], axis=0
+            )
+            source = tok[kind, zb] if k > 0 else (rows, cots)[kind][...]
+            found = jnp.dot(picks.astype(bf16), source, preferred_element_type=f32)
+            if kind == 1:
+                table = jnp.concatenate(
+                    [
+                        jnp.broadcast_to(meta[zb, pl.ds(n_sp + e, 1), :], (capacity, tokens))
+                        for e in (s, beside)
+                    ],
+                    axis=0,
+                )
+                found = found * jnp.sum(picks * table, axis=1, keepdims=True)
+            found = found.astype(bf16)
+            ybuf[kind, zb] = found[capacity:]
+            got[kind, window(block, capacity), window(t, width)] = found[:capacity]
+            for copy in sends:
+                copy.start()
+
+        if valid is None:
+            work()
+        else:
+            pl.when(valid)(work)
+
+    def hear(distance, kind):
+        for k in range(1, n_z):
+            apart = {abs(found[k] - place) for place, found in enumerate(nearest(n_z))}
+            if distance not in apart:
+                continue
+            zb = order[k]
+            only = None if len(apart) == 1 else abs_of(zb - z) == distance
+            waits = [move_tokens(kind, zb, z, 0, False)] + [move_meta(zb, z, 0)] * (kind == 0)
+            for copy in waits:
+                if only is None:
+                    copy.wait_recv()
+                else:
+                    pl.when(only)(copy.wait_recv)
+            make = [lambda zb, to, way: move_tokens(kind, zb, to, way, False)]
+            for made in make + [move_meta] * (kind == 0):
+                above, below = (zb < z) & (z + 1 < n_z), (zb > z) & (z >= 1)
+                if only is not None:
+                    above, below = above & only, below & only
+                begin(made(zb, z + 1, 0), above)
+                begin(made(zb, z - 1, 1), below)
+        for k in range(1, n_z):
+            apart = {abs(found[k] - place) for place, found in enumerate(nearest(n_z))}
+            if distance in apart:
+                only = None if len(apart) == 1 else abs_of(order[k] - z) == distance
+                compact(kind, k, only)
+
+    def take_beside(kind, k):
+        block = order[k] * n_y + 1 - y
+        from_beside(kind, order[k]).wait_recv()
+        begin(share(kind, block, 2))
+        begin(share(kind, block, 1))
+
+    def gather_chunk(k):
+        blocks = [order[k] * n_y + y, order[k] * n_y + 1 - y]
+        for block in blocks:
+            for kind in range(2):
+                arrived(kind, block, 2).wait_recv()
+                begin(share(kind, block, 3))
+        for block in blocks:
+            for kind in range(2):
+                arrived(kind, block, 1).wait_recv()
+                arrived(kind, block, 3).wait_recv()
+
+    def to_pair(zb, slot):
+        here = window(zb, chunk)
+        return remote(
+            give_pair.at[slot, here], half.at[slot, here],
+            pss.at[zb, slot], prs.at[zb, slot], (s, pair),
+        )
+
+    def cross(zb):
+        here = window(zb, chunk)
+        return remote(xsend.at[here], xrecv.at[here], css.at[zb], crs.at[zb], (s, across))
+
+    def give(block):
+        here = window(block, capacity)
+        return remote(
+            back.at[here], ret.at[window(s, capacity)], gss.at[block], grs.at[s], (block, t)
+        )
+
+    def given(source):
+        here = window(source, capacity)
+        return remote(back.at[here], ret.at[here], gss.at[source], grs.at[source], (source, t))
+
+    def experts(k):
+        zb = order[k]
+        here = window(zb, chunk)
+        got_rows = got[0, here, :]
+        pre_gate = jnp.dot(got_rows, w_gate[...], preferred_element_type=f32)
+        pre_up = jnp.dot(got_rows, w_up[...], preferred_element_type=f32)
+        d_active = contract_columns(got[1, here, :], w_down[...])
+        gate_act, slope = silu_parts(pre_gate)
+        act[here, :] = (gate_act * pre_up).astype(bf16)
+        d_gate = (d_active * pre_up * slope).astype(bf16)
+        d_up = (d_active * gate_act).astype(bf16)
+        dgate[here, :] = d_gate
+        dup[here, :] = d_up
+
+        def partial(quarter):
+            columns = window(quarter, width)
+            return contract_columns(d_gate, w_gate[columns, :]) + contract_columns(
+                d_up, w_up[columns, :]
+            )
+
+        give_pair[0, here, :] = partial(flip(pair, 2)).astype(bf16)
+        begin(to_pair(zb, 0))
+        give_pair[1, here, :] = partial(pair).astype(bf16)
+        begin(to_pair(zb, 1))
+        mine[0, here, :] = partial(across)
+        mine[1, here, :] = partial(t)
+
+    def send_across(k):
+        zb = order[k]
+        here = window(zb, chunk)
+        to_pair(zb, 0).wait_recv()
+        xsend[here, :] = (mine[0, here, :] + half[0, here, :].astype(f32)).astype(bf16)
+        begin(cross(zb))
+
+    def send_home(k):
+        zb = order[k]
+        here = window(zb, chunk)
+        to_pair(zb, 1).wait_recv()
+        cross(zb).wait_recv()
+        total = (
+            mine[1, here, :] + half[1, here, :].astype(f32) + xrecv[here, :].astype(f32)
+        ).astype(bf16)
+        back[here, :] = total
+        if k > 0:
+            begin(give(zb * n_y + y))
+        else:
+            ret[window(s, capacity), :] = back[window(s, capacity), :]
+        begin(give(zb * n_y + 1 - y))
+
+    step = 256 if width % 256 == 0 else width
+
+    def weight_grad(target, kind, right):
+        def lap(j, _):
+            columns = window(j, step)
+            target[columns, :] = contract_rows(got[kind, :, columns], right[...]).astype(bf16)
+            return 0
+
+        lax.fori_loop(0, n_tp * width // step, lap, 0)
+
+    def down_grad():
+        def lap(j, _):
+            columns = window(j, step)
+            grad_down[:, columns] = contract_rows(act[...], got[1, :, columns]).astype(bf16)
+            return 0
+
+        lax.fori_loop(0, n_tp * width // step, lap, 0)
+
+    def take_mixed(k):
+        zb = order[k]
+        if k == 0:
+            spread(lambda zb, to, way: move_mixed(zb, to, way, True), zb, True)
+        else:
+            move_mixed(zb, z, 0, False).wait_recv()
+            spread(lambda zb, to, way: move_mixed(zb, to, way, False), zb, False)
+        begin(mixed_beside(zb, k == 0))
+
+    def share_out(k):
+        bit = low_bit(k)
+        ref = out.at[:, window(flip(t, k - bit), width)]
+        return remote(ref, ref, oss.at[k], ors.at[k], (s, flip(t, bit)))
+
+    def out_arrived(k):
+        ref = out.at[:, window(flip(t, k), width)]
+        return remote(ref, ref, oss.at[k], ors.at[k], (s, flip(t, low_bit(k))))
+
+    strip = 16
+
+    def recurrence():
+        def lap(j, _):
+            here = window(j, strip)
+            rate_row = rate[...]
+            recur_f = recur[here, :].astype(f32)
+            input_f = inputs[here, :].astype(f32)
+            conv_f = conv[here, :].astype(f32)
+            before_f = before[here, :].astype(f32)
+            gate_f = gate_pre[here, :].astype(f32)
+            log_decay = -8.0 * recur_f * rate_row
+            decay_now = jnp.exp(log_decay)
+            place = lax.broadcasted_iota(jnp.int32, conv_f.shape, 0) + (s * tokens + j * strip)
+            at_start = place == 0
+            norm = jnp.where(at_start, 1.0, jnp.sqrt(-expm1_of(2.0 * log_decay)))
+            slope = jnp.where(at_start, 0.0, -jnp.exp(2.0 * log_decay) / norm)
+            entry = input_f * conv_f
+            kept = decay_now * before_f
+            state = kept + norm * entry
+            inner = 0.7978845608028654 * (gate_f + 0.044715 * gate_f * gate_f * gate_f)
+            bend = jnp.tanh(inner)
+            half_up = 0.5 * (1.0 + bend)
+            gate_now = gate_f * half_up
+            gate_slope = half_up + 0.5 * gate_f * (1.0 - bend * bend) * 0.7978845608028654 * (
+                1.0 + 3.0 * 0.044715 * gate_f * gate_f
+            )
+            decay[here, :] = decay_now
+            gate[here, :] = gate_now
+            gate_part[here, :] = state * gate_slope
+            mixed[here, :] = (state * gate_now).astype(bf16)
+            recur_part[here, :] = (
+                (kept + slope * entry) * (-8.0 * rate_row) * recur_f * (1.0 - recur_f)
+            )
+            input_part[here, :] = norm * conv_f * input_f * (1.0 - input_f)
+            conv_part[here, :] = norm * input_f
+            return 0
+
+        lax.fori_loop(0, tokens // strip, lap, 0)
+
+        def back_lap(step, held):
+            row = tokens - 1 - step
+            product[pl.ds(row, 1), :] = held
+            return held * decay[pl.ds(row, 1), :]
+
+        one = jnp.ones((1, width), f32)
+        carry[0:1, :] = lax.fori_loop(0, tokens, back_lap, one, unroll=8)
+
+    cut = n_tp * width // n_sp
+    held_blocks = width // cut
+
+    def piece(q, t_to):
+        columns = window(q, cut)
+        return remote(
+            out.at[:, columns], pieces.at[s], iss.at[q, lax.div(t_to, 2)], irs.at[s], (q, t_to)
+        )
+
+    def piece_beside(block):
+        return remote(
+            pieces.at[block], pieces.at[block], kss.at[block], irs.at[block], (s, pair)
+        )
+
+    def send_carry(m):
+        return remote(carry, carries.at[s], krs.at[0, m], krs.at[1, m], (flip(s, m), t))
+
+    for kind in range(2):
+        compact(kind, 0)
+    for expert in range(n_sp):
+        pick[expert * capacity : (expert + 1) * capacity, :] = (
+            chosen(z, expert).astype(f32).astype(bf16)
+        )
+    for kind in range(2):
+        take_beside(kind, 0)
+    for distance in range(1, n_z):
+        hear(distance, 0)
+        if distance == 1:
+            hear(distance, 1)
+            take_beside(0, 1)
+            for copy in fetch[4:]:
+                copy.wait()
+            recurrence()
+            own_mixed = pltpu.make_async_copy(mixed, mixed_all.at[s], own_sem)
+            own_mixed.start()
+            continue
+        take_beside(1, distance - 1)
+        gather_chunk(distance - 2)
+        experts(distance - 2)
+        hear(distance, 1)
+        take_beside(0, distance)
+    take_mixed(0)
+    take_beside(1, n_z - 1)
+    for k in range(n_z - 2, n_z):
+        gather_chunk(k)
+        experts(k)
+        if k < n_z - 1:
+            take_mixed(1)
+        if k == n_z - 2:
+            for earlier_k in range(1, n_z - 1):
+                send_across(earlier_k)
+    send_across(n_z - 1)
+    send_across(0)
+    for k in range(2, n_z):
+        take_mixed(k)
+    for k in range(1, n_z - 1):
+        send_home(k)
+    down_grad()
+    send_home(n_z - 1)
+    weight_grad(grad_gate, 0, dgate)
+    send_home(0)
+    weight_grad(grad_up, 0, dup)
+    for m in range(1, n_sp):
+        given(flip(s, m)).wait_recv()
+    total = cots[...].astype(f32) + contract_rows(pick[...], ret[...])
+    out[:, window(t, width)] = total.astype(bf16)
+    begin(share_out(2))
+    begin(share_out(1))
+    for j in range(held_blocks):
+        q = t * held_blocks + j
+        begin(piece(q, t), abs_of(q - s) > 0)
+        begin(piece(q, across), abs_of(q - s) > 0)
+
+    def through_proj(k):
+        columns = window(flip(t, k), width)
+        return jnp.dot(out[:, columns], proj[columns, :], preferred_element_type=f32)
+
+    drive[...] = through_proj(0)
+    out_arrived(1).wait_recv()
+    drive[...] += through_proj(1)
+    out_arrived(2).wait_recv()
+    begin(share_out(3))
+    drive[...] += through_proj(2)
+    out_arrived(3).wait_recv()
+    d_mixed = drive[...] + through_proj(3)
+    grad_gate_pre[...] = (d_mixed * gate_part[...]).astype(bf16)
+    drive[...] = d_mixed * gate[...]
+
+    def lap(step, held):
+        row = tokens - 1 - step
+        grad = drive[pl.ds(row, 1), :] + held
+        state_grad[pl.ds(row, 1), :] = grad
+        return decay[pl.ds(row, 1), :] * grad
+
+    zero = jnp.zeros((1, width), f32)
+    carry[1:2, :] = lax.fori_loop(0, tokens, lap, zero, unroll=8)
+    for m in range(1, n_sp):
+        begin(send_carry(m))
+    own_piece = out[:, window(s, cut)]
+    pieces[s] = own_piece
+    direct = lax.rem(lax.div(s, held_blocks), 2) == lax.rem(t, 2)
+    for m in range(1, n_sp):
+        block = flip(s, m)
+        pl.when(direct)(piece_beside(block).wait_recv)
+        begin(piece_beside(block), direct)
+    for m in range(1, n_sp):
+        send_carry(m).wait_recv()
+    incoming = zero
+    for later in range(n_sp - 1, 0, -1):
+        longer = carries[later, 1:2, :] + carries[later, 0:1, :] * incoming
+        incoming = jnp.where(later > s, longer, incoming)
+    state_grad[...] = state_grad[...] + product[...] * incoming
+    for m in range(1, n_sp):
+        pl.when(jnp.logical_not(direct))(piece_beside(flip(s, m)).wait_recv)
+    for k in range(n_z):
+        mixed_from_beside(order[k]).wait_recv()
+    own_mixed.wait()
+    for copy, valid in ends:
+        if valid is None:
+            copy.wait_send()
+        else:
+            pl.when(valid)(copy.wait_send)
+
+
+def finish_kernel(
+    mixed_all, pieces, grad_gate, grad_up, grad_down, state_grad, recur_part, input_part,
+    conv_part, grad_gate_pre, recur_hbm, input_hbm,
+    out_gate, out_up, out_down, out_proj, out_conv, out_gate_pre,
+    recur_map, input_map, proj_block, conv_block, sems,
+):
+    loads = [
+        pltpu.make_async_copy(recur_hbm, recur_map, sems.at[0]),
+        pltpu.make_async_copy(input_hbm, input_map, sems.at[1]),
+    ]
+    for copy in loads:
+        copy.start()
+    ready = (
+        (grad_gate, out_gate), (grad_up, out_up), (grad_down, out_down),
+        (grad_gate_pre, out_gate_pre),
+    )
+    stores = [pltpu.make_async_copy(a, b, sems.at[2 + i]) for i, (a, b) in enumerate(ready)]
+    for copy in stores:
+        copy.start()
+    bf16 = jnp.bfloat16
+    proj_block[...] = contract_rows(pieces[...], mixed_all[...])
+    stores.append(pltpu.make_async_copy(proj_block, out_proj, sems.at[6]))
+    stores[-1].start()
+    grad = state_grad[...]
+    d_recur = (grad * recur_part[...]).astype(bf16)
+    d_input = (grad * input_part[...]).astype(bf16)
+    for copy in loads:
+        copy.wait()
+    width = recur_map.shape[1]
+    for group in range(recur_map.shape[0]):
+        columns = slice(group * width, (group + 1) * width)
+        through = contract_columns(d_recur[:, columns], recur_map[group])
+        through = through + contract_columns(d_input[:, columns], input_map[group])
+        conv_block[:, columns] = (
+            state_grad[:, columns] * conv_part[:, columns] + through
+        ).astype(bf16)
+    stores.append(pltpu.make_async_copy(conv_block, out_conv, sems.at[7]))
+    stores[-1].start()
+    for copy in stores:
+        copy.wait()
+
+
+def run_dense(experts, tps, capacity, maps, *operands):
+    row_block, w_gate = operands[0], operands[11]
+    tokens, width = row_block.shape
+    features = tps * width
+    hidden = w_gate.shape[1]
+    slots, n_z = experts * capacity, experts // 2
+    bf16, f32 = jnp.bfloat16, jnp.float32
+    outer = pl.BlockSpec(memory_space=pltpu.HBM)
+    tile, wide = (tokens, width), (tokens, features)
+    cut = features // experts
+    weight, down = (features, hidden), (hidden, features)
+    struct = jax.ShapeDtypeStruct
+    results = [
+        struct((experts, tokens, width), bf16),
+        struct((experts, tokens, cut), bf16),
+        struct(weight, bf16),
+        struct(weight, bf16),
+        struct(down, bf16),
+        struct(tile, f32),
+        struct(tile, f32),
+        struct(tile, f32),
+        struct(tile, f32),
+        struct(tile, bf16),
+    ]
+    done = pl.pallas_call(
+        functools.partial(expert_kernel, experts, tps, capacity),
+        out_shape=results,
+        in_specs=[outer] * len(operands),
+        out_specs=[VMEM] * len(results),
+        scratch_shapes=[pltpu.VMEM(operand.shape, operand.dtype) for operand in operands]
+        + [
+            pltpu.VMEM((2, n_z, *tile), bf16),
+            pltpu.VMEM((n_z, 2 * experts, tokens), f32),
+            pltpu.VMEM((2, slots, features), bf16),
+            pltpu.VMEM((2, n_z, capacity, width), bf16),
+            pltpu.VMEM((slots, hidden), bf16),
+            pltpu.VMEM((slots, hidden), bf16),
+            pltpu.VMEM((slots, hidden), bf16),
+            pltpu.VMEM((2, slots, width), bf16),
+            pltpu.VMEM((2, slots, width), f32),
+            pltpu.VMEM((2, slots, width), bf16),
+            pltpu.VMEM((slots, width), bf16),
+            pltpu.VMEM((slots, width), bf16),
+            pltpu.VMEM((slots, width), bf16),
+            pltpu.VMEM((slots, width), bf16),
+            pltpu.VMEM((slots, tokens), bf16),
+            pltpu.VMEM(wide, bf16),
+            pltpu.VMEM(tile, bf16),
+            pltpu.VMEM(tile, f32),
+            pltpu.VMEM(tile, f32),
+            pltpu.VMEM(tile, f32),
+            pltpu.VMEM(tile, f32),
+            pltpu.VMEM(tile, f32),
+            pltpu.VMEM((2, width), f32),
+            pltpu.VMEM((experts, 2, width), f32),
+            DMA((len(operands),)),
+            DMA((2, n_z, 2)),
+            DMA((2, n_z)),
+            DMA((n_z, 2)),
+            DMA((n_z,)),
+            DMA((2, n_z)),
+            DMA((2, n_z)),
+            DMA((2, experts, tps)),
+            DMA((2, experts, tps)),
+            DMA((n_z, 2)),
+            DMA((n_z, 2)),
+            DMA((n_z,)),
+            DMA((n_z,)),
+            DMA((experts,)),
+            DMA((experts,)),
+            DMA((n_z, 3)),
+            DMA((experts,)),
+            DMA((tps,)),
+            DMA((tps,)),
+            DMA((experts, 2)),
+            DMA((experts,)),
+            DMA((experts,)),
+            DMA((2, experts)),
+            DMA,
+        ],
+        compiler_params=pltpu.CompilerParams(
+            collective_id=3, has_side_effects=True, vmem_limit_bytes=32 * 1024 * 1024
+        ),
+    )(*[pltpu.with_memory_space_constraint(each, pltpu.HBM) for each in operands])
+    mixed_all, pieces, *others = done
+    everything = [
+        mixed_all.reshape(experts * tokens, width), pieces.reshape(experts * tokens, cut), *others,
+    ]
+    finals = [
+        struct(weight, bf16),
+        struct(weight, bf16),
+        struct(down, bf16),
+        struct((cut, width), f32),
+        struct(tile, bf16),
+        struct(tile, bf16),
+    ]
+    return pl.pallas_call(
+        finish_kernel,
+        out_shape=finals,
+        in_specs=[VMEM] * len(everything) + [outer] * 2,
+        out_specs=[outer] * len(finals),
+        scratch_shapes=[pltpu.VMEM(each.shape, each.dtype) for each in maps]
+        + [pltpu.VMEM((cut, width), f32), pltpu.VMEM(tile, bf16), DMA((8,))],
+        compiler_params=pltpu.CompilerParams(vmem_limit_bytes=16 * 1024 * 1024),
+    )(*everything, *[pltpu.with_memory_space_constraint(each, pltpu.HBM) for each in maps])
 
 
 def dispatch_kernel(n_sp, n_tp, rows, cots, got_rows, got_cots, own_sem, sa, ra, st, rt):
@@ -322,7 +987,7 @@
     )
 
 
-def body(
+def sparse_body(
     cotangent,
     mixer_out,
     route_ids,
@@ -498,6 +1163,76 @@
     )
 
 
+def body(
+    cotangent,
+    mixer_out,
+    route_ids,
+    route_weights,
+    conv_out,
+    recur_gate,
+    input_gate,
+    gate_pre,
+    states_before,
+    decay_rate,
+    out_proj,
+    recur_map,
+    input_map,
+    expert_gate,
+    expert_up,
+    expert_down,
+):
+    experts, tps = lax.axis_size("sp"), lax.axis_size("tp")
+    row_count = cotangent.shape[0]
+    capacity = 4 * row_count // experts
+    if 2 * capacity < row_count:
+        return sparse_body(
+            cotangent,
+            mixer_out,
+            route_ids,
+            route_weights,
+            conv_out,
+            recur_gate,
+            input_gate,
+            gate_pre,
+            states_before,
+            decay_rate,
+            out_proj,
+            recur_map,
+            input_map,
+            expert_gate,
+            expert_up,
+            expert_down,
+        )
+    grad_gate, grad_up, grad_down, grad_out_proj, grad_conv, grad_gate_pre = run_dense(
+        experts,
+        tps,
+        capacity,
+        (recur_map, input_map),
+        mixer_out,
+        cotangent,
+        route_ids.T,
+        route_weights.T,
+        conv_out,
+        recur_gate,
+        input_gate,
+        gate_pre,
+        states_before,
+        decay_rate[None, :],
+        out_proj,
+        expert_gate[0],
+        expert_up[0],
+        expert_down[0],
+    )
+    return (
+        grad_gate[None],
+        grad_up[None],
+        grad_down[None],
+        grad_out_proj,
+        grad_conv,
+        grad_gate_pre,
+    )
+
+
 def solution(mesh):
     placed = (
         P("sp", "tp"),

time: 111 us -> 75.3 us (0.68)
  matrix products: 18.1 us -> 0 us
  Pallas kernels: 83.1 us -> 74.5 us
  local copies, waits for them, and re-layouts: 6.31 us -> 0 us
  other arithmetic: 2.09 us -> 0 us
    dot_general x14 -> x0, matrix products: 18.1 us -> none  [the longest x3 5.21 us: contract_rows(): lax.dot_general(left, right, (((0,), (0,)), ((), ())), preferred_element_...]
    pallas_call x3 -> x2, Pallas kernels: 83.1 us -> 74.5 us  [the longest x1 71.2 us: run_dense(): pl.pallas_call(functools.partial(expert_kernel, experts, tps, capacity),...]
    unnamed x37 -> x0, local copies, waits for them, and re-layouts: 4.58 us -> none
where the time goes in v1:
time: 75.3 us; the launch traced here: 75.2 us
  Pallas kernels  74.5 us (99%)
    pallas_call x1, Pallas kernels, run_dense(): pl.pallas_call(functools.partial(expert_kernel, experts, tps, capacity),...  71.2 us
    pallas_call x1, Pallas kernels, run_dense(): pl.pallas_call(finish_kernel, out_shape=finals, in_specs=[VMEM] * len(eve...  3.37 us

profile of v1, /device:TPU:0, one launch (start us, length us, event | category | flops | bytes accessed | tf_op | source)
XLA Modules:
  0.0 75.2 jit_solution(14946192655575168047)
XLA Ops:
  0.6 71.2 %shard_map.199 = (bf16[8,128,512]{2,1,0:T(8,128)(2,1)S(1)}, bf16[8,128,256]{2,1,0:T(8,128)(2,1)S(1)}, bf16[2048,256]{1,0:T(8,128)(2,1)S(1)}, bf16[2048,256]{1,0:...) custom-call(bf16[128,512]{1,0:T(8,128)(2,1)} %rows_hbm.1, ...), custom_call_target="tpu_custom_call" | custom-call | tf_op jit(solution)/shard_map/pallas_call | solution.py:658
  71.8 3.4 %shard_map.200 = (bf16[2048,256]{1,0:T(8,128)(2,1)}, bf16[2048,256]{1,0:T(8,128)(2,1)}, bf16[256,2048]{1,0:T(8,128)(2,1)}, f32[256,512]{1,0:T(8,128)}, bf16[128,...) custom-call(bf16[1024,512]{1,0:T(8,128)(2,1)S(1)} %bitcast.11, bf16[1024,256]{1,0:T(8,128)(2,1)S(1)} %bitcast.12, ...), custom_call_target="tpu_custom_call" | custom-call | tf_op jit(solution)/shard_map/pallas_call | solution.py:730

commit v2 on v1

--- a/solution.py
+++ b/solution.py
@@ -104,15 +104,15 @@
 def expert_kernel(
     n_sp, n_tp, capacity,
     rows_hbm, cots_hbm, ids_hbm, weights_hbm, conv_hbm, recur_hbm, input_hbm, gate_hbm,
-    before_hbm, rate_hbm, proj_hbm, w_gate_hbm, w_up_hbm, w_down_hbm,
-    mixed_all, pieces, grad_gate, grad_up, grad_down, state_grad, recur_part, input_part,
-    conv_part, grad_gate_pre,
+    before_hbm, rate_hbm, proj_hbm, w_gate_hbm, w_up_hbm, w_down_hbm, recur_map_hbm,
+    input_map_hbm,
+    proj_block, grad_gate, grad_up, grad_down, grad_conv, grad_gate_pre,
     rows, cots, ids, weights, conv, recur, inputs, gate_pre, before, rate, proj,
-    w_gate, w_up, w_down,
+    w_gate, w_up, w_down, recur_map, input_map,
     tok, meta, got, ybuf, act, dgate, dup, give_pair, mine, half,
-    xsend, xrecv, back, ret, pick, out, mixed, decay, gate, gate_part, drive, product, carry,
-    carries,
-    lsem, tss, trs, mss, mrs, yss, yrs, hss, hrs, pss, prs, css, crs, gss, grs,
+    xsend, xrecv, back, ret, pick, mixed_all, pieces, out, mixed, decay, gate, gate_part, drive, product,
+    state_grad, recur_part, input_part, conv_part, carry, carries,
+    lsem, tss, trs, mss, mrs, yss, yrs, hss, hrs, hds, pss, prs, css, crs, gss, grs,
     zss, zrs, oss, ors, iss, irs, kss, krs, own_sem,
 ):
     s, t = lax.axis_index("sp"), lax.axis_index("tp")
@@ -134,6 +134,7 @@
                 (conv_hbm, conv), (recur_hbm, recur), (input_hbm, inputs), (gate_hbm, gate_pre),
                 (before_hbm, before), (rate_hbm, rate),
                 (w_gate_hbm, w_gate), (w_up_hbm, w_up), (w_down_hbm, w_down), (proj_hbm, proj),
+                (recur_map_hbm, recur_map), (input_map_hbm, input_map),
             )
         )
     ]
@@ -146,8 +147,9 @@
         copy.wait()
     ends = []
 
-    def begin(copy, valid=None):
-        ends.append((copy, valid))
+    def begin(copy, valid=None, alone=True):
+        if alone:
+            ends.append((copy, valid))
         if valid is None:
             copy.start()
         else:
@@ -191,25 +193,24 @@
     def to_beside(kind, zb):
         return remote(
             ybuf.at[kind, zb], slots(kind, zb * n_y + y, t),
-            yss.at[kind, zb], yrs.at[kind, zb], (beside, t),
+            yss, yrs.at[kind, zb], (beside, t),
         )
 
     def from_beside(kind, zb):
         return remote(
             ybuf.at[kind, zb], slots(kind, zb * n_y + 1 - y, t),
-            yss.at[kind, zb], yrs.at[kind, zb], (beside, t),
+            yss, yrs.at[kind, zb], (beside, t),
         )
 
     def share(kind, block, k):
         bit = low_bit(k)
         ref = slots(kind, block, flip(t, k - bit))
-        return remote(ref, ref, hss.at[kind, block, k], hrs.at[kind, block, k], (s, flip(t, bit)))
-
-    def arrived(kind, block, k):
-        ref = slots(kind, block, flip(t, k))
-        return remote(
-            ref, ref, hss.at[kind, block, k], hrs.at[kind, block, k], (s, flip(t, low_bit(k)))
-        )
+        recv_sem = hrs.at[kind, block] if k == 2 else hds.at[lax.div(block, n_y)]
+        return remote(ref, ref, hss, recv_sem, (s, flip(t, bit)))
+
+    def crossed(kind, block):
+        ref = slots(kind, block, across)
+        return remote(ref, ref, hss, hrs.at[kind, block], (s, across))
 
     table_rows = lax.broadcasted_iota(jnp.int32, (2 * n_sp, tokens), 0)
     first_id, second_id = ids[0:1, :], ids[1:2, :]
@@ -240,7 +241,6 @@
         zb = order[k]
         block = zb * n_y + y
         sends = (to_beside(kind, zb), share(kind, block, 2), share(kind, block, 1))
-        ends.extend((copy, valid) for copy in sends)
 
         def work():
             picks = jnp.concatenate(
@@ -297,40 +297,38 @@
     def take_beside(kind, k):
         block = order[k] * n_y + 1 - y
         from_beside(kind, order[k]).wait_recv()
-        begin(share(kind, block, 2))
-        begin(share(kind, block, 1))
+        begin(share(kind, block, 2), alone=False)
+        begin(share(kind, block, 1), alone=False)
+
+    def relay_x(kind, k):
+        for block in (order[k] * n_y + y, order[k] * n_y + 1 - y):
+            crossed(kind, block).wait_recv()
+            begin(share(kind, block, 3), alone=False)
 
     def gather_chunk(k):
-        blocks = [order[k] * n_y + y, order[k] * n_y + 1 - y]
-        for block in blocks:
-            for kind in range(2):
-                arrived(kind, block, 2).wait_recv()
-                begin(share(kind, block, 3))
-        for block in blocks:
-            for kind in range(2):
-                arrived(kind, block, 1).wait_recv()
-                arrived(kind, block, 3).wait_recv()
+        both = got.at[:, window(order[k], chunk), pl.ds(0, (n_tp // 2) * width)]
+        remote(both, both, hss, hds.at[order[k]], (s, pair)).wait_recv()
 
     def to_pair(zb, slot):
         here = window(zb, chunk)
         return remote(
             give_pair.at[slot, here], half.at[slot, here],
-            pss.at[zb, slot], prs.at[zb, slot], (s, pair),
+            pss, prs.at[zb, slot], (s, pair),
         )
 
     def cross(zb):
         here = window(zb, chunk)
-        return remote(xsend.at[here], xrecv.at[here], css.at[zb], crs.at[zb], (s, across))
+        return remote(xsend.at[here], xrecv.at[here], css, crs.at[zb], (s, across))
 
     def give(block):
         here = window(block, capacity)
         return remote(
-            back.at[here], ret.at[window(s, capacity)], gss.at[block], grs.at[s], (block, t)
+            back.at[here], ret.at[window(s, capacity)], gss, grs, (block, t)
         )
 
-    def given(source):
-        here = window(source, capacity)
-        return remote(back.at[here], ret.at[here], gss.at[source], grs.at[source], (source, t))
+    def given():
+        most = pl.ds(0, (n_sp - 1) * capacity)
+        return remote(back.at[most], ret.at[most], gss, grs, (beside, t))
 
     def experts(k):
         zb = order[k]
@@ -353,9 +351,9 @@
             )
 
         give_pair[0, here, :] = partial(flip(pair, 2)).astype(bf16)
-        begin(to_pair(zb, 0))
+        begin(to_pair(zb, 0), alone=False)
         give_pair[1, here, :] = partial(pair).astype(bf16)
-        begin(to_pair(zb, 1))
+        begin(to_pair(zb, 1), alone=False)
         mine[0, here, :] = partial(across)
         mine[1, here, :] = partial(t)
 
@@ -364,7 +362,7 @@
         here = window(zb, chunk)
         to_pair(zb, 0).wait_recv()
         xsend[here, :] = (mine[0, here, :] + half[0, here, :].astype(f32)).astype(bf16)
-        begin(cross(zb))
+        begin(cross(zb), alone=False)
 
     def send_home(k):
         zb = order[k]
@@ -376,10 +374,10 @@
         ).astype(bf16)
         back[here, :] = total
         if k > 0:
-            begin(give(zb * n_y + y))
+            begin(give(zb * n_y + y), alone=False)
         else:
             ret[window(s, capacity), :] = back[window(s, capacity), :]
-        begin(give(zb * n_y + 1 - y))
+        begin(give(zb * n_y + 1 - y), alone=False)
 
     step = 256 if width % 256 == 0 else width
 
@@ -399,23 +397,37 @@
 
         lax.fori_loop(0, n_tp * width // step, lap, 0)
 
-    def take_mixed(k):
-        zb = order[k]
-        if k == 0:
-            spread(lambda zb, to, way: move_mixed(zb, to, way, True), zb, True)
-        else:
-            move_mixed(zb, z, 0, False).wait_recv()
-            spread(lambda zb, to, way: move_mixed(zb, to, way, False), zb, False)
-        begin(mixed_beside(zb, k == 0))
+    def send_mixed():
+        spread(lambda zb, to, way: move_mixed(zb, to, way, True), z, True)
+        begin(mixed_beside(z, True))
+
+    def take_mixed(distance):
+        for k in range(1, n_z):
+            apart = {abs(found[k] - place) for place, found in enumerate(nearest(n_z))}
+            if distance not in apart:
+                continue
+            zb = order[k]
+            only = None if len(apart) == 1 else abs_of(zb - z) == distance
+            wait = move_mixed(zb, z, 0, False).wait_recv
+            if only is None:
+                wait()
+            else:
+                pl.when(only)(wait)
+            above, below = (zb < z) & (z + 1 < n_z), (zb > z) & (z >= 1)
+            if only is not None:
+                above, below = above & only, below & only
+            begin(move_mixed(zb, z + 1, 0, False), above)
+            begin(move_mixed(zb, z - 1, 1, False), below)
+            begin(mixed_beside(zb, False), only)
 
     def share_out(k):
         bit = low_bit(k)
         ref = out.at[:, window(flip(t, k - bit), width)]
-        return remote(ref, ref, oss.at[k], ors.at[k], (s, flip(t, bit)))
+        return remote(ref, ref, oss, ors.at[k - 1], (s, flip(t, bit)))
 
     def out_arrived(k):
         ref = out.at[:, window(flip(t, k), width)]
-        return remote(ref, ref, oss.at[k], ors.at[k], (s, flip(t, low_bit(k))))
+        return remote(ref, ref, oss, ors.at[k - 1], (s, flip(t, low_bit(k))))
 
     strip = 16
 
@@ -468,15 +480,16 @@
     cut = n_tp * width // n_sp
     held_blocks = width // cut
 
-    def piece(q, t_to):
-        columns = window(q, cut)
+    def piece(j, way):
+        q = t * held_blocks + j
         return remote(
-            out.at[:, columns], pieces.at[s], iss.at[q, lax.div(t_to, 2)], irs.at[s], (q, t_to)
+            out.at[:, window(q, cut)], pieces.at[s], iss.at[j, way], irs.at[s],
+            (q, across if way else t),
         )
 
     def piece_beside(block):
         return remote(
-            pieces.at[block], pieces.at[block], kss.at[block], irs.at[block], (s, pair)
+            pieces.at[block], pieces.at[block], kss, irs.at[block], (s, pair)
         )
 
     def send_carry(m):
@@ -490,53 +503,59 @@
         )
     for kind in range(2):
         take_beside(kind, 0)
-    for distance in range(1, n_z):
+    hear(1, 0)
+    hear(1, 1)
+    take_beside(0, 1)
+    for copy in fetch[4:]:
+        copy.wait()
+    recurrence()
+    own_mixed = pltpu.make_async_copy(mixed, mixed_all.at[s], own_sem)
+    own_mixed.start()
+    relay_x(0, 0)
+    relay_x(1, 0)
+    for distance in range(2, n_z):
         hear(distance, 0)
-        if distance == 1:
-            hear(distance, 1)
-            take_beside(0, 1)
-            for copy in fetch[4:]:
-                copy.wait()
-            recurrence()
-            own_mixed = pltpu.make_async_copy(mixed, mixed_all.at[s], own_sem)
-            own_mixed.start()
-            continue
         take_beside(1, distance - 1)
+        hear(distance, 1)
+        if distance == n_z - 2:
+            send_mixed()
         gather_chunk(distance - 2)
         experts(distance - 2)
-        hear(distance, 1)
         take_beside(0, distance)
-    take_mixed(0)
+        for kind in range(2):
+            relay_x(kind, distance - 1)
     take_beside(1, n_z - 1)
+    send_across(0)
     for k in range(n_z - 2, n_z):
         gather_chunk(k)
         experts(k)
-        if k < n_z - 1:
+        if k == n_z - 2:
+            for kind in range(2):
+                relay_x(kind, n_z - 1)
             take_mixed(1)
-        if k == n_z - 2:
-            for earlier_k in range(1, n_z - 1):
-                send_across(earlier_k)
-    send_across(n_z - 1)
-    send_across(0)
-    for k in range(2, n_z):
-        take_mixed(k)
-    for k in range(1, n_z - 1):
-        send_home(k)
+        send_across(k)
+    for distance in range(2, n_z - 1):
+        take_mixed(distance)
+    send_home(n_z - 2)
+    for k in range(1, n_z - 2):
+        send_across(k)
+    send_home(0)
     down_grad()
     send_home(n_z - 1)
     weight_grad(grad_gate, 0, dgate)
-    send_home(0)
+    for k in range(1, n_z - 2):
+        send_home(k)
     weight_grad(grad_up, 0, dup)
-    for m in range(1, n_sp):
-        given(flip(s, m)).wait_recv()
+    take_mixed(n_z - 1)
+    given().wait_recv()
     total = cots[...].astype(f32) + contract_rows(pick[...], ret[...])
     out[:, window(t, width)] = total.astype(bf16)
-    begin(share_out(2))
-    begin(share_out(1))
+    begin(share_out(2), alone=False)
+    begin(share_out(1), alone=False)
     for j in range(held_blocks):
         q = t * held_blocks + j
-        begin(piece(q, t), abs_of(q - s) > 0)
-        begin(piece(q, across), abs_of(q - s) > 0)
+        begin(piece(j, 0), abs_of(q - s) > 0)
+        begin(piece(j, 1), abs_of(q - s) > 0)
 
     def through_proj(k):
         columns = window(flip(t, k), width)
@@ -546,7 +565,7 @@
     out_arrived(1).wait_recv()
     drive[...] += through_proj(1)
     out_arrived(2).wait_recv()
-    begin(share_out(3))
+    begin(share_out(3), alone=False)
     drive[...] += through_proj(2)
     out_arrived(3).wait_recv()
     d_mixed = drive[...] + through_proj(3)
@@ -561,27 +580,48 @@
 
     zero = jnp.zeros((1, width), f32)
     carry[1:2, :] = lax.fori_loop(0, tokens, lap, zero, unroll=8)
+    direct = lax.rem(lax.div(s, held_blocks), 2) == lax.rem(t, 2)
     for m in range(1, n_sp):
-        begin(send_carry(m))
-    own_piece = out[:, window(s, cut)]
-    pieces[s] = own_piece
-    direct = lax.rem(lax.div(s, held_blocks), 2) == lax.rem(t, 2)
+        begin(send_carry(m), flip(s, m) < s)
+    pieces[s] = out[:, window(s, cut)]
     for m in range(1, n_sp):
         block = flip(s, m)
         pl.when(direct)(piece_beside(block).wait_recv)
-        begin(piece_beside(block), direct)
+        begin(piece_beside(block), direct, alone=False)
+    for k in range(n_z):
+        mixed_from_beside(order[k]).wait_recv()
+    own_mixed.wait()
     for m in range(1, n_sp):
-        send_carry(m).wait_recv()
+        pl.when(jnp.logical_not(direct))(piece_beside(flip(s, m)).wait_recv)
+    proj_block[...] = contract_rows(
+        pieces[...].reshape(n_sp * tokens, cut), mixed_all[...].reshape(n_sp * tokens, width)
+    )
+    for m in range(1, n_sp):
+        pl.when(flip(s, m) > s)(send_carry(m).wait_recv)
     incoming = zero
     for later in range(n_sp - 1, 0, -1):
         longer = carries[later, 1:2, :] + carries[later, 0:1, :] * incoming
         incoming = jnp.where(later > s, longer, incoming)
-    state_grad[...] = state_grad[...] + product[...] * incoming
-    for m in range(1, n_sp):
-        pl.when(jnp.logical_not(direct))(piece_beside(flip(s, m)).wait_recv)
-    for k in range(n_z):
-        mixed_from_beside(order[k]).wait_recv()
-    own_mixed.wait()
+    grad = state_grad[...] + product[...] * incoming
+    d_recur = (grad * recur_part[...]).astype(bf16)
+    d_input = (grad * input_part[...]).astype(bf16)
+    straight = grad * conv_part[...]
+    side = recur_map.shape[1]
+    for group in range(recur_map.shape[0]):
+        columns = slice(group * side, (group + 1) * side)
+        through = contract_columns(d_recur[:, columns], recur_map[group])
+        through = through + contract_columns(d_input[:, columns], input_map[group])
+        grad_conv[:, columns] = (straight[:, columns] + through).astype(bf16)
+    some = got.at[:, pl.ds(0, (n_tp - 1) * chunk), :]
+    remote(some, some, hss, hds.at[0], (s, pair)).wait_send()
+    remote(ybuf, ybuf, yss, yrs.at[0, 0], (beside, t)).wait_send()
+    remote(give_pair, half, pss, prs.at[0, 0], (s, pair)).wait_send()
+    remote(xsend, xrecv, css, crs.at[0], (s, across)).wait_send()
+    given().wait_send()
+    others = out.at[:, pl.ds(0, (n_tp - 1) * width)]
+    remote(others, others, oss, ors.at[0], (s, pair)).wait_send()
+    spare = pieces.at[pl.ds(0, n_sp - 1)]
+    pl.when(direct)(remote(spare, spare, kss, irs.at[0], (s, pair)).wait_send)
     for copy, valid in ends:
         if valid is None:
             copy.wait_send()
@@ -589,49 +629,19 @@
             pl.when(valid)(copy.wait_send)
 
 
-def finish_kernel(
-    mixed_all, pieces, grad_gate, grad_up, grad_down, state_grad, recur_part, input_part,
-    conv_part, grad_gate_pre, recur_hbm, input_hbm,
-    out_gate, out_up, out_down, out_proj, out_conv, out_gate_pre,
-    recur_map, input_map, proj_block, conv_block, sems,
-):
-    loads = [
-        pltpu.make_async_copy(recur_hbm, recur_map, sems.at[0]),
-        pltpu.make_async_copy(input_hbm, input_map, sems.at[1]),
+def finish_kernel(*refs):
+    count = len(refs) // 2
+    sems = refs[-1]
+    stores = [
+        pltpu.make_async_copy(refs[i], refs[count + i], sems.at[i]) for i in range(count)
     ]
-    for copy in loads:
-        copy.start()
-    ready = (
-        (grad_gate, out_gate), (grad_up, out_up), (grad_down, out_down),
-        (grad_gate_pre, out_gate_pre),
-    )
-    stores = [pltpu.make_async_copy(a, b, sems.at[2 + i]) for i, (a, b) in enumerate(ready)]
     for copy in stores:
         copy.start()
-    bf16 = jnp.bfloat16
-    proj_block[...] = contract_rows(pieces[...], mixed_all[...])
-    stores.append(pltpu.make_async_copy(proj_block, out_proj, sems.at[6]))
-    stores[-1].start()
-    grad = state_grad[...]
-    d_recur = (grad * recur_part[...]).astype(bf16)
-    d_input = (grad * input_part[...]).astype(bf16)
-    for copy in loads:
-        copy.wait()
-    width = recur_map.shape[1]
-    for group in range(recur_map.shape[0]):
-        columns = slice(group * width, (group + 1) * width)
-        through = contract_columns(d_recur[:, columns], recur_map[group])
-        through = through + contract_columns(d_input[:, columns], input_map[group])
-        conv_block[:, columns] = (
-            state_grad[:, columns] * conv_part[:, columns] + through
-        ).astype(bf16)
-    stores.append(pltpu.make_async_copy(conv_block, out_conv, sems.at[7]))
-    stores[-1].start()
     for copy in stores:
         copy.wait()
 
 
-def run_dense(experts, tps, capacity, maps, *operands):
+def run_dense(experts, tps, capacity, *operands):
     row_block, w_gate = operands[0], operands[11]
     tokens, width = row_block.shape
     features = tps * width
@@ -644,15 +654,11 @@
     weight, down = (features, hidden), (hidden, features)
     struct = jax.ShapeDtypeStruct
     results = [
-        struct((experts, tokens, width), bf16),
-        struct((experts, tokens, cut), bf16),
+        struct((cut, width), f32),
         struct(weight, bf16),
         struct(weight, bf16),
         struct(down, bf16),
-        struct(tile, f32),
-        struct(tile, f32),
-        struct(tile, f32),
-        struct(tile, f32),
+        struct(tile, bf16),
         struct(tile, bf16),
     ]
     done = pl.pallas_call(
@@ -677,8 +683,14 @@
             pltpu.VMEM((slots, width), bf16),
             pltpu.VMEM((slots, width), bf16),
             pltpu.VMEM((slots, tokens), bf16),
+            pltpu.VMEM((experts, tokens, width), bf16),
+            pltpu.VMEM((experts, tokens, cut), bf16),
             pltpu.VMEM(wide, bf16),
             pltpu.VMEM(tile, bf16),
+            pltpu.VMEM(tile, f32),
+            pltpu.VMEM(tile, f32),
+            pltpu.VMEM(tile, f32),
+            pltpu.VMEM(tile, f32),
             pltpu.VMEM(tile, f32),
             pltpu.VMEM(tile, f32),
             pltpu.VMEM(tile, f32),
@@ -691,23 +703,24 @@
             DMA((2, n_z)),
             DMA((n_z, 2)),
             DMA((n_z,)),
+            DMA,
             DMA((2, n_z)),
-            DMA((2, n_z)),
-            DMA((2, experts, tps)),
-            DMA((2, experts, tps)),
+            DMA,
+            DMA((2, experts)),
+            DMA((n_z,)),
+            DMA,
             DMA((n_z, 2)),
-            DMA((n_z, 2)),
+            DMA,
             DMA((n_z,)),
-            DMA((n_z,)),
-            DMA((experts,)),
-            DMA((experts,)),
+            DMA,
+            DMA,
             DMA((n_z, 3)),
             DMA((experts,)),
-            DMA((tps,)),
-            DMA((tps,)),
-            DMA((experts, 2)),
+            DMA,
+            DMA((tps - 1,)),
+            DMA((experts // tps, 2)),
             DMA((experts,)),
-            DMA((experts,)),
+            DMA,
             DMA((2, experts)),
             DMA,
         ],
@@ -715,27 +728,14 @@
             collective_id=3, has_side_effects=True, vmem_limit_bytes=32 * 1024 * 1024
         ),
     )(*[pltpu.with_memory_space_constraint(each, pltpu.HBM) for each in operands])
-    mixed_all, pieces, *others = done
-    everything = [
-        mixed_all.reshape(experts * tokens, width), pieces.reshape(experts * tokens, cut), *others,
-    ]
-    finals = [
-        struct(weight, bf16),
-        struct(weight, bf16),
-        struct(down, bf16),
-        struct((cut, width), f32),
-        struct(tile, bf16),
-        struct(tile, bf16),
-    ]
     return pl.pallas_call(
         finish_kernel,
-        out_shape=finals,
-        in_specs=[VMEM] * len(everything) + [outer] * 2,
-        out_specs=[outer] * len(finals),
-        scratch_shapes=[pltpu.VMEM(each.shape, each.dtype) for each in maps]
-        + [pltpu.VMEM((cut, width), f32), pltpu.VMEM(tile, bf16), DMA((8,))],
+        out_shape=results,
+        in_specs=[VMEM] * len(results),
+        out_specs=[outer] * len(results),
+        scratch_shapes=[DMA((len(results),))],
         compiler_params=pltpu.CompilerParams(vmem_limit_bytes=16 * 1024 * 1024),
-    )(*everything, *[pltpu.with_memory_space_constraint(each, pltpu.HBM) for each in maps])
+    )(*done)
 
 
 def dispatch_kernel(n_sp, n_tp, rows, cots, got_rows, got_cots, own_sem, sa, ra, st, rt):
@@ -1203,11 +1203,10 @@
             expert_up,
             expert_down,
         )
-    grad_gate, grad_up, grad_down, grad_out_proj, grad_conv, grad_gate_pre = run_dense(
+    grad_out_proj, grad_gate, grad_up, grad_down, grad_conv, grad_gate_pre = run_dense(
         experts,
         tps,
         capacity,
-        (recur_map, input_map),
         mixer_out,
         cotangent,
         route_ids.T,
@@ -1222,6 +1221,8 @@
         expert_gate[0],
         expert_up[0],
         expert_down[0],
+        recur_map,
+        input_map,
     )
     return (
         grad_gate[None],

time: 75.3 us -> 69.7 us (0.926)
  Pallas kernels: 74.5 us -> 68.2 us
    pallas_call x1, Pallas kernels: 71.2 us -> 66.3 us  [run_dense(): pl.pallas_call(functools.partial(expert_kernel, experts, tps, capacity),...]
    pallas_call x1, Pallas kernels: 3.37 us -> 1.96 us  [run_dense(): pl.pallas_call(finish_kernel, out_shape=results, in_specs=[VMEM] * len(re...]
where the time goes in v2:
time: 69.7 us; the launch traced here: 68.9 us
  Pallas kernels  68.2 us (98%)
    pallas_call x1, Pallas kernels, run_dense(): pl.pallas_call(functools.partial(expert_kernel, experts, tps, capacity),...  66.3 us
    pallas_call x1, Pallas kernels, run_dense(): pl.pallas_call(finish_kernel, out_shape=results, in_specs=[VMEM] * len(re...  1.96 us

profile of v2, /device:TPU:0, one launch (start us, length us, event | category | flops | bytes accessed | tf_op | source)
XLA Modules:
  0.0 68.9 jit_solution(13977163215388157046)
XLA Ops:
  0.6 66.3 %shard_map.199 = (f32[256,512]{1,0:T(8,128)S(1)}, bf16[2048,256]{1,0:T(8,128)(2,1)S(1)}, bf16[2048,256]{1,0:T(8,128)(2,1)S(1)}, bf16[256,2048]{1,0:T(8,128)(2,1)...) custom-call(bf16[128,512]{1,0:T(8,128)(2,1)} %rows_hbm.1, bf16[128,512]{1,0:T(8,128)(2,1)} %cots_hbm.1, ...), custom_call_target="tpu_custom_call" | custom-call | tf_op jit(solution)/shard_map/pallas_call | solution.py:664
  66.9 2.0 %shard_map.200 = (f32[256,512]{1,0:T(8,128)}, bf16[2048,256]{1,0:T(8,128)(2,1)}, bf16[2048,256]{1,0:T(8,128)(2,1)}, bf16[256,2048]{1,0:T(8,128)(2,1)}, bf16[128,...) custom-call(f32[256,512]{1,0:T(8,128)S(1)} %get-tuple-element.18.refs_0_, bf16[2048,256]{1,0:T(8,128)(2,1)S(1)} %get-tuple-element.19.refs_1_, ...), custom_call_target="tpu_custom_call" | custom-call | tf_op jit(solution)/shard_map/pallas_call | solution.py:731

commit v3 on v2

--- a/solution.py
+++ b/solution.py
@@ -519,12 +519,14 @@
         hear(distance, 1)
         if distance == n_z - 2:
             send_mixed()
-        gather_chunk(distance - 2)
-        experts(distance - 2)
+        if distance == 2:
+            gather_chunk(0)
+            experts(0)
         take_beside(0, distance)
         for kind in range(2):
             relay_x(kind, distance - 1)
     take_beside(1, n_z - 1)
+    take_mixed(1)
     send_across(0)
     for k in range(n_z - 2, n_z):
         gather_chunk(k)
@@ -532,19 +534,20 @@
         if k == n_z - 2:
             for kind in range(2):
                 relay_x(kind, n_z - 1)
-            take_mixed(1)
         send_across(k)
     for distance in range(2, n_z - 1):
         take_mixed(distance)
     send_home(n_z - 2)
+    send_home(0)
     for k in range(1, n_z - 2):
+        gather_chunk(k)
+        experts(k)
         send_across(k)
-    send_home(0)
+    send_home(n_z - 1)
     down_grad()
-    send_home(n_z - 1)
-    weight_grad(grad_gate, 0, dgate)
     for k in range(1, n_z - 2):
         send_home(k)
+    weight_grad(grad_gate, 0, dgate)
     weight_grad(grad_up, 0, dup)
     take_mixed(n_z - 1)
     given().wait_recv()

time: 69.7 us -> 69.3 us (level)
  no operation moved by 1% of the time
where the time goes in v3:
time: 69.3 us; the launch traced here: 68.8 us
  Pallas kernels  68.1 us (98%)
    pallas_call x1, Pallas kernels, run_dense(): pl.pallas_call(functools.partial(expert_kernel, experts, tps, capacity),...  66.2 us
    pallas_call x1, Pallas kernels, run_dense(): pl.pallas_call(finish_kernel, out_shape=results, in_specs=[VMEM] * len(re...  1.96 us

profile of v3, /device:TPU:0, one launch (start us, length us, event | category | flops | bytes accessed | tf_op | source)
XLA Modules:
  0.0 68.8 jit_solution(2378432112562533445)
XLA Ops:
  0.6 66.2 %shard_map.199 = (f32[256,512]{1,0:T(8,128)S(1)}, bf16[2048,256]{1,0:T(8,128)(2,1)S(1)}, bf16[2048,256]{1,0:T(8,128)(2,1)S(1)}, bf16[256,2048]{1,0:T(8,128)(2,1)...) custom-call(bf16[128,512]{1,0:T(8,128)(2,1)} %rows_hbm.1, bf16[128,512]{1,0:T(8,128)(2,1)} %cots_hbm.1, ...), custom_call_target="tpu_custom_call" | custom-call | tf_op jit(solution)/shard_map/pallas_call | solution.py:667
  66.8 2.0 %shard_map.200 = (f32[256,512]{1,0:T(8,128)}, bf16[2048,256]{1,0:T(8,128)(2,1)}, bf16[2048,256]{1,0:T(8,128)(2,1)}, bf16[256,2048]{1,0:T(8,128)(2,1)}, bf16[128,...) custom-call(f32[256,512]{1,0:T(8,128)S(1)} %get-tuple-element.18.refs_0_, bf16[2048,256]{1,0:T(8,128)(2,1)S(1)} %get-tuple-element.19.refs_1_, ...), custom_call_target="tpu_custom_call" | custom-call | tf_op jit(solution)/shard_map/pallas_call | solution.py:734
